TPU v7x, 256 devices: a whole 4x4x8 slice. The times are simulated.
256 devices in a mesh: ep: 64 (over z, y, core), tp: 4 (over x).
Axes of the slice: x: 4, y: 4, z: 8, core: 2. Of those that a mesh axis runs over, the one named last changes fastest.
Arguments:
- tokens: bfloat16 [1024, 2048], P('ep'), may hold values from -6 to 6
- norm_gain: bfloat16 [2048], replicated, may hold values from 0.099609375 to 1.8984375
- query_weight: bfloat16 [2048, 1024], P('ep', 'tp'), may hold values from -0.125 to 0.125
- key_weight: bfloat16 [2048, 1024], P('ep', 'tp'), may hold values from -0.125 to 0.125
- value_weight: bfloat16 [2048, 2048], P('ep', 'tp'), may hold values from -0.125 to 0.125
- outgate_weight: bfloat16 [2048, 2048], P('ep', 'tp'), may hold values from -0.125 to 0.125
- beta_weight: bfloat16 [2048, 16], replicated, may hold values from -0.125 to 0.125
- decay_weight: bfloat16 [2048, 16], replicated, may hold values from -0.125 to 0.125
- decay_rate: float32 [16], P('tp'), may hold values from 0.02 to 6
- decay_bias: float32 [16], P('tp'), may hold values from -3 to 3
- head_gain: bfloat16 [128], replicated, may hold values from 0.099609375 to 1.8984375
- recurrent: float32 [1024, 16, 128, 128], P('ep', 'tp'), may hold values from -3 to 3
- output_weight: bfloat16 [2048, 2048], P('tp', 'ep'), may hold values from -0.125 to 0.125
- ffn_gain: bfloat16 [2048], replicated, may hold values from 0.099609375 to 1.8984375
- routes: int32 [1024, 4], P('ep'), may hold values from 0 to 63, all different within a row; in each aligned block of 16 rows (0 to 15, 16 to 31, ...) at most 2 rows name the same one
- route_weight: float32 [1024, 4], P('ep'), may hold values from 0.1 to 1
- expert_gate: bfloat16 [64, 2048, 512], P('ep', None, 'tp'), may hold values from -0.125 to 0.125
- expert_up: bfloat16 [64, 2048, 512], P('ep', None, 'tp'), may hold values from -0.125 to 0.125
- expert_down: bfloat16 [64, 512, 2048], P('ep', 'tp'), may hold values from -0.25 to 0.25
- shared_gate: bfloat16 [2048, 512], P('ep', 'tp'), may hold values from -0.125 to 0.125
- shared_up: bfloat16 [2048, 512], P('ep', 'tp'), may hold values from -0.125 to 0.125
- shared_down: bfloat16 [512, 2048], P('tp', 'ep'), may hold values from -0.25 to 0.25
- branch_gate: bfloat16 [2048], replicated, may hold values from -0.125 to 0.125
Outputs:
- layer_out: bfloat16 [1024, 2048], P('ep')
- new_state: float32 [1024, 16, 128, 128], P('ep', 'tp')
Inputs may be any that keep to these rules, and one draw needn't show every extreme that they name: `routes`: each row names 4 different experts. Among the rows of one aligned block of 16 rows no expert is named more than 2 times, and some block reaches it: one expert is named exactly 2 times there.
All inputs are finite; a program needn't handle non-finite values.
Results may differ from a plain program's by a relative error of at most 0.019.
Values may be sent and summed in bfloat16 or wider, within the bound.
No kernel may reach another device: no remote copies, remote signals or barrier semaphores. Data moves between devices by JAX's collectives and lax.ppermute only.
A program may use at most 64 MiB of HBM per device.

v0:
```python
import jax
import jax.numpy as jnp
from jax import lax
from jax.sharding import PartitionSpec as P

EPS = 1e-06
ROUTED_SCALE = 2.5


def side_by_side(arrays, axis, dim, along):
    both = jnp.concatenate(arrays, axis=along)
    whole, at, outs = (lax.all_gather(both, axis, axis=dim, tiled=True), 0, [])
    for a in arrays:
        outs.append(lax.slice_in_dim(whole, at, at + a.shape[along], axis=along))
        at += a.shape[along]
    return tuple(outs)


def copy_for_each(array, axis):
    copies = jnp.broadcast_to(array, (lax.axis_size(axis), *array.shape))
    return lax.all_to_all(copies, axis, split_axis=0, concat_axis=0, tiled=True)


def laid_out(pieces, dim):
    dims = list(pieces.shape[1:])
    dims[dim] *= pieces.shape[0]
    return jnp.moveaxis(pieces, 0, dim).reshape(dims)


def collect(array, axis, dim):
    pieces = copy_for_each(array, axis)
    return laid_out(pieces, dim)


def over_copies(array, axis):
    everything = copy_for_each(array, axis)
    return jnp.sum(everything.astype(jnp.float32), axis=0)


def in_blocks(array, dim, peers):
    dims = array.shape
    pieces = array.reshape(*dims[:dim], peers, dims[dim] // peers, *dims[dim + 1 :])
    return jnp.moveaxis(pieces, dim, 0)


def summed_on_arrival(array, axis, dim):
    pieces = in_blocks(array, dim, lax.axis_size(axis))
    arrived = lax.all_to_all(pieces, axis, split_axis=0, concat_axis=0, tiled=True)
    return arrived.astype(jnp.float32).sum(axis=0)


def rms_scale(values, gain):
    values = values.astype(jnp.float32)
    return (
        values
        * lax.rsqrt(jnp.mean(values * values, axis=-1, keepdims=True) + EPS)
        * gain.astype(jnp.float32)
    )


def unit_rows(values):
    return values * lax.rsqrt(jnp.sum(values * values, axis=-1, keepdims=True) + EPS)


def per_device(
    tokens,
    norm_gain,
    query_weight,
    key_weight,
    value_weight,
    outgate_weight,
    beta_weight,
    decay_weight,
    decay_rate,
    decay_bias,
    head_gain,
    recurrent,
    output_weight,
    ffn_gain,
    routes,
    route_weight,
    expert_gate,
    expert_up,
    expert_down,
    shared_gate,
    shared_up,
    shared_down,
    branch_gate,
):
    ep_count = lax.axis_size("ep")
    tp_count = lax.axis_size("tp")
    seq_local, width = tokens.shape
    heads_local, key_dim, value_dim = (recurrent.shape[1], recurrent.shape[2], recurrent.shape[3])
    normed = rms_scale(tokens, norm_gain).astype(jnp.bfloat16)
    query_cols = query_weight.shape[1]
    pieces = side_by_side((query_weight, key_weight, value_weight, outgate_weight), "ep", 0, 1)
    token_block = normed
    query_sum, key_sum, value_sum, gate_sum = tuple(
        (
            jnp.dot(token_block, weight_piece, preferred_element_type=jnp.float32)
            for weight_piece in pieces
        )
    )
    query_proj = query_sum.astype(jnp.bfloat16)
    key_proj = key_sum.astype(jnp.bfloat16)
    value_proj = value_sum.astype(jnp.bfloat16)
    gate_proj = gate_sum.astype(jnp.bfloat16)
    key_local = query_cols // key_dim
    repeat_count = heads_local // key_local
    queries = unit_rows(
        jax.nn.silu(query_proj.astype(jnp.float32)).reshape(seq_local, key_local, key_dim)
    )
    queries = jnp.repeat(queries, repeat_count, axis=1) * key_dim ** (-0.5)
    key_rows = unit_rows(
        jax.nn.silu(key_proj.astype(jnp.float32)).reshape(seq_local, key_local, key_dim)
    )
    key_rows = jnp.repeat(key_rows, repeat_count, axis=1)
    value_rows = jax.nn.silu(value_proj.astype(jnp.float32)).reshape(
        seq_local, heads_local, value_dim
    )
    head_start = lax.axis_index("tp") * heads_local
    beta_logit = jnp.dot(
        normed,
        lax.dynamic_slice_in_dim(beta_weight, head_start, heads_local, 1),
        preferred_element_type=jnp.float32,
    )
    decay_logit = jnp.dot(
        normed,
        lax.dynamic_slice_in_dim(decay_weight, head_start, heads_local, 1),
        preferred_element_type=jnp.float32,
    )
    strength = jax.nn.sigmoid(beta_logit)
    retain = jnp.exp(-decay_rate[None, :] * jax.nn.softplus(decay_logit + decay_bias[None, :]))
    decayed = recurrent * retain[:, :, None, None]
    predicted = jnp.einsum("shde,shd->she", decayed, key_rows)
    correction = strength[:, :, None] * (value_rows - predicted)
    new_state = decayed + key_rows[:, :, :, None] * correction[:, :, None, :]
    readout = jnp.einsum("shde,shd->she", new_state, queries)
    out_gate = jax.nn.silu(gate_proj.astype(jnp.float32)).reshape(seq_local, heads_local, value_dim)
    heads_out = (
        (rms_scale(readout, head_gain) * out_gate)
        .astype(jnp.bfloat16)
        .reshape(seq_local, heads_local * value_dim)
    )
    partial_mix = jnp.dot(
        heads_out, collect(output_weight, "ep", 1), preferred_element_type=jnp.float32
    )
    partial_mix = partial_mix.astype(jnp.bfloat16).astype(jnp.float32)
    mixed = over_copies(partial_mix.astype(jnp.bfloat16), "tp").astype(jnp.float32)
    residual = (tokens.astype(jnp.float32) + mixed).astype(jnp.bfloat16)
    ffn_in = rms_scale(residual, ffn_gain).astype(jnp.bfloat16)
    pieces = side_by_side((shared_gate, shared_up), "ep", 0, 1)
    token_block = ffn_in
    shared_g = jnp.dot(token_block, pieces[0], preferred_element_type=jnp.float32)
    shared_u = jnp.dot(token_block, pieces[1], preferred_element_type=jnp.float32)
    shared_act = (jax.nn.silu(shared_g) * shared_u).astype(jnp.bfloat16)
    shared_partial = jnp.dot(
        shared_act, collect(shared_down, "ep", 1), preferred_element_type=jnp.float32
    )
    shared_out = over_copies(
        shared_partial.astype(jnp.bfloat16).astype(jnp.float32).astype(jnp.bfloat16), "tp"
    ).astype(jnp.float32)
    topk = routes.shape[1]
    pair_count = seq_local * topk
    capacity = 2 * ((pair_count + ep_count - 1) // ep_count)
    expert_ids = routes.reshape(pair_count)
    onehot = (expert_ids[:, None] == jnp.arange(ep_count)[None, :]).astype(jnp.float32)
    earlier = (jnp.arange(pair_count)[:, None] > jnp.arange(pair_count)[None, :]).astype(
        jnp.float32
    )
    slots = jnp.sum(jnp.dot(earlier, onehot) * onehot, axis=1).astype(jnp.int32)
    target = expert_ids * capacity + slots
    placement_matrix = (target[:, None] == jnp.arange(ep_count * capacity)[None, :]).astype(
        jnp.bfloat16
    )
    dispatch_matrix = jnp.sum(
        placement_matrix.reshape(seq_local, topk, ep_count * capacity).astype(jnp.float32), axis=1
    ).astype(jnp.bfloat16)
    outgoing = jnp.dot(dispatch_matrix.T, ffn_in, preferred_element_type=jnp.float32).astype(
        jnp.bfloat16
    )
    outgoing = outgoing.reshape(ep_count, capacity, width)
    share_cols = width // tp_count
    received = lax.all_to_all(outgoing, "ep", split_axis=0, concat_axis=0, tiled=True)
    flat_rows = received.reshape(-1, width)
    gate_part = jnp.dot(flat_rows, expert_gate[0], preferred_element_type=jnp.float32)
    up_part = jnp.dot(flat_rows, expert_up[0], preferred_element_type=jnp.float32)
    act = (jax.nn.silu(gate_part) * up_part).astype(jnp.bfloat16)
    partial_rows = (
        jnp.dot(act, expert_down[0], preferred_element_type=jnp.float32)
        .astype(jnp.bfloat16)
        .astype(jnp.float32)
    )
    part_cols = summed_on_arrival(partial_rows.astype(jnp.bfloat16), "tp", 1).astype(jnp.bfloat16)
    returned = lax.all_to_all(
        part_cols.reshape(received.shape[0], received.shape[1], share_cols),
        "ep",
        split_axis=0,
        concat_axis=0,
        tiled=True,
    )
    scaled = route_weight / jnp.sum(route_weight, axis=1, keepdims=True) * ROUTED_SCALE
    branch = jax.nn.sigmoid(jnp.dot(ffn_in, branch_gate, preferred_element_type=jnp.float32))
    col_begin = lax.axis_index("tp") * share_cols
    pair_out = jnp.dot(
        placement_matrix,
        returned.reshape(ep_count * capacity, share_cols),
        preferred_element_type=jnp.float32,
    )
    moe_cols = jnp.sum(pair_out.reshape(seq_local, topk, share_cols) * scaled[:, :, None], axis=1)
    resid_part = lax.dynamic_slice_in_dim(residual, col_begin, share_cols, 1).astype(jnp.float32)
    shared_part = lax.dynamic_slice_in_dim(shared_out, col_begin, share_cols, 1)
    out_cols = (resid_part + moe_cols + branch[:, None] * shared_part).astype(jnp.bfloat16)
    layer_out = collect(out_cols, "tp", 1)
    return (layer_out, new_state)


def solution(mesh):
    return jax.shard_map(
        per_device,
        mesh=mesh,
        in_specs=(
            P("ep", None),
            P(),
            P("ep", "tp"),
            P("ep", "tp"),
            P("ep", "tp"),
            P("ep", "tp"),
            P(),
            P(),
            P("tp"),
            P("tp"),
            P(),
            P("ep", "tp", None, None),
            P("tp", "ep"),
            P(),
            P("ep", None),
            P("ep", None),
            P("ep", None, "tp"),
            P("ep", None, "tp"),
            P("ep", "tp", None),
            P("ep", "tp"),
            P("ep", "tp"),
            P("tp", "ep"),
            P(),
        ),
        out_specs=(P("ep", None), P("ep", "tp", None, None)),
        check_vma=False,
    )
```

profile of v0, /device:TPU:1, one launch (start us, length us, event | category | flops | bytes accessed | tf_op | source)
XLA Modules:
  0.0 266.9 jit_solution(13242425956207793846)
XLA Ops:
  8.8 2.3 broadcast_in_dim.16
  11.1 13.1 %all-to-all-start = ((bf16[64,512,32]{1,2,0:T(8,128)(2,1)}), bf16[64,512,32]{1,2,0:T(8,128)(2,1)S(1)}, u32[]{:S(2)}, u32[]{:S(2)}) async-start(bf16[64,512,32]{1,2,0:T(8,128)(2,1)} %broadcast_in_dim.16), calls=%async_computation | async-start | bytes 4194304 | tf_op jit(solution)/shard_map/all_to_all | solution.py:21
  27.2 74.0 %all-gather.3.cloned.1.call-done = bf16[2048,1536]{1,0:T(8,128)(2,1)} async-done(((bf16[32,1536]{1,0:T(8,128)(2,1)}), bf16[2048,1536]{1,0:T(8,128)(2,1)}) %all-gather.3.cloned.1.call-update) | async-done | bytes 6291472 | tf_op jit(solution)/shard_map/all_gather | solution.py:12
  101.1 1.5 divide_multiply_fusion.2
  102.7 1.5 divide_multiply_fusion.3
  104.2 2.0 divide_multiply_fusion.1
  106.3 2.0 divide_multiply_fusion
  108.8 3.1 %fusion = f32[16,4,1,128]{3,2,1,0:T(1,128)S(1)} fusion(f32[16,4,128,1]{2,3,1,0:T(1,128)S(1)} %bitcast.70, f32[16,4,128,128]{3,2,1,0:T(8,128)} %param.34, f32[16,4]{1,0:T(8,128)S(1)} %copy.58), kind=kOutput, calls=%fused_computation.1 | convolution fusion | flops 3145728 | bytes 4260096 | tf_op jit(solution)/shard_map/shde,shd->she/dot_general | solution.py:135
  113.5 2.0 copy-done.2
  117.8 3.9 %all-to-all-start.1 = ((bf16[4,16,2048]{2,1,0:T(8,128)(2,1)}), bf16[4,16,2048]{2,1,0:T(8,128)(2,1)S(1)}, u32[]{:S(2)}, u32[]{:S(2)}) async-start(bf16[4,16,2048]{2,1,0:T(8,128)(2,1)} %broadcast_in_dim.17), calls=%async_computation.1 | async-start | bytes 524288 | tf_op jit(solution)/shard_map/all_to_all | solution.py:21
  121.7 5.8 %all-to-all-done.1 = bf16[4,16,2048]{2,1,0:T(8,128)(2,1)S(1)} async-done(((bf16[4,16,2048]{2,1,0:T(8,128)(2,1)}), bf16[4,16,2048]{2,1,0:T(8,128)(2,1)S(1)}, u32[]{:S(2)}, u32[]{:S(2)}) %all-to-all-start.1) | async-done | bytes 262176 | tf_op jit(solution)/shard_map/all_to_all | solution.py:21
  129.3 9.7 %all-to-all-start.2 = ((bf16[64,2,2048]{2,1,0:T(2,128)(2,1)}), bf16[64,2,2048]{2,1,0:T(2,128)(2,1)S(1)}, u32[]{:S(2)}, u32[]{:S(2)}) async-start(bf16[64,2,2048]{2,1,0:T(2,128)(2,1)} %reshape.147), calls=%async_computation.2 | async-start | bytes 1048576 | tf_op jit(solution)/shard_map/all_to_all | solution.py:184
  139.8 16.9 %all-to-all-done.2 = bf16[64,2,2048]{2,1,0:T(2,128)(2,1)S(1)} async-done(((bf16[64,2,2048]{2,1,0:T(2,128)(2,1)}), bf16[64,2,2048]{2,1,0:T(2,128)(2,1)S(1)}, u32[]{:S(2)}, u32[]{:S(2)}) %all-to-all-start.2) | async-done | bytes 524320 | tf_op jit(solution)/shard_map/all_to_all | solution.py:184
  157.6 5.7 %all-to-all-start.5 = ((bf16[64,128,32]{1,2,0:T(8,128)(2,1)}), bf16[64,128,32]{1,2,0:T(8,128)(2,1)S(1)}, u32[]{:S(2)}, u32[]{:S(2)}) async-start(bf16[64,128,32]{1,2,0:T(8,128)(2,1)} %broadcast_in_dim.18), calls=%async_computation.5 | async-start | bytes 1048576 | tf_op jit(solution)/shard_map/all_to_all | solution.py:21
  163.8 1.6 convolution_convert_fusion
  166.3 15.0 %all-to-all-done.5 = bf16[64,128,32]{1,2,0:T(8,128)(2,1)S(1)} async-done(((bf16[64,128,32]{1,2,0:T(8,128)(2,1)}), bf16[64,128,32]{1,2,0:T(8,128)(2,1)S(1)}, u32[]{:S(2)}, u32[]{:S(2)}) %all-to-all-start.5) | async-done | bytes 524320 | tf_op jit(solution)/shard_map/all_to_all | solution.py:21
  181.3 3.5 %all-to-all-start.3 = ((bf16[4,128,512]{2,1,0:T(8,128)(2,1)}), bf16[4,128,512]{2,1,0:T(8,128)(2,1)S(1)}, u32[]{:S(2)}, u32[]{:S(2)}) async-start(bf16[4,128,512]{2,1,0:T(8,128)(2,1)} %bitcast.66), calls=%async_computation.3 | async-start | bytes 1048576 | tf_op jit(solution)/shard_map/all_to_all | solution.py:48
  184.7 34.9 %all-gather.5.cloned.1.call-done = bf16[2048,256]{1,0:T(8,128)(2,1)} async-done(((bf16[32,256]{1,0:T(8,128)(2,1)}), bf16[2048,256]{1,0:T(8,128)(2,1)}) %all-gather.5.cloned.1.call-update) | async-done | bytes 1048592 | tf_op jit(solution)/shard_map/all_gather | solution.py:12
  220.9 1.5 convolution_convert_fusion.2
  223.1 4.0 %all-to-all-start.6 = ((bf16[4,16,2048]{2,1,0:T(8,128)(2,1)}), bf16[4,16,2048]{2,1,0:T(8,128)(2,1)S(1)}, u32[]{:S(2)}, u32[]{:S(2)}) async-start(bf16[4,16,2048]{2,1,0:T(8,128)(2,1)} %broadcast_in_dim.19), calls=%async_computation.6 | async-start | bytes 524288 | tf_op jit(solution)/shard_map/all_to_all | solution.py:21
  227.9 5.1 %all-to-all-done.6 = bf16[4,16,2048]{2,1,0:T(8,128)(2,1)S(1)} async-done(((bf16[4,16,2048]{2,1,0:T(8,128)(2,1)}), bf16[4,16,2048]{2,1,0:T(8,128)(2,1)S(1)}, u32[]{:S(2)}, u32[]{:S(2)}) %all-to-all-start.6) | async-done | bytes 262176 | tf_op jit(solution)/shard_map/all_to_all | solution.py:21
  233.0 8.2 %all-to-all-start.4 = ((bf16[64,2,512]{2,1,0:T(2,128)(2,1)}), bf16[64,2,512]{2,1,0:T(2,128)(2,1)S(1)}, u32[]{:S(2)}, u32[]{:S(2)}) async-start(bf16[64,2,512]{2,1,0:T(2,128)(2,1)} %reshape.150), calls=%async_computation.4 | async-start | bytes 262144 | tf_op jit(solution)/shard_map/all_to_all | solution.py:195
  241.4 10.8 %all-to-all-done.4 = bf16[64,2,512]{2,1,0:T(2,128)(2,1)S(1)} async-done(((bf16[64,2,512]{2,1,0:T(2,128)(2,1)}), bf16[64,2,512]{2,1,0:T(2,128)(2,1)S(1)}, u32[]{:S(2)}, u32[]{:S(2)}) %all-to-all-start.4) | async-done | bytes 131104 | tf_op jit(solution)/shard_map/all_to_all | solution.py:195
  252.6 6.8 %all_to_all.40 = bf16[4,16,512]{2,1,0:T(8,128)(2,1)S(1)} all-to-all(bf16[4,16,512]{2,1,0:T(8,128)(2,1)S(1)} %broadcast_in_dim.20), channel_id=1, replica_groups=mesh['ep'=64,'tp'=4] {'tp'}, dimensions={0} | all-to-all | bytes 131072 | tf_op jit(solution)/shard_map/all_to_all | solution.py:21
  (100 shorter events, 17.4 us)
Async XLA Ops:
  7.2 156.7 %copy-start = (bf16[1,128,2048]{2,1,0:T(8,128)(2,1)S(1)}, bf16[1,128,2048]{2,1,0:T(8,128)(2,1)}, u32[]{:S(2)}) copy-start(bf16[1,128,2048]{2,1,0:T(8,128)(2,1)} %param.41) | copy-start | bytes 1572868
  7.2 17.1 %copy-start.13 = (f32[4]{0:T(128)S(1)}, f32[4]{0:T(128)}, u32[]{:S(2)}) copy-start(f32[4]{0:T(128)} %param.31) | copy-start | bytes 52
  7.2 17.1 %copy-start.10 = (bf16[2048]{0:T(1024)(128)(2,1)S(1)}, bf16[2048]{0:T(1024)(128)(2,1)}, u32[]{:S(2)}) copy-start(bf16[2048]{0:T(1024)(128)(2,1)} %param.24) | copy-start | bytes 12292
  7.2 17.1 %copy-start.6 = (s32[16,4]{0,1:T(4,128)S(1)}, s32[16,4]{0,1:T(4,128)}, u32[]{:S(2)}) copy-start(s32[16,4]{0,1:T(4,128)} %param.37) | copy-start | bytes 772
  7.2 17.3 %copy-start.4 = (bf16[16,2048]{1,0:T(8,128)(2,1)S(1)}, bf16[16,2048]{1,0:T(8,128)(2,1)}, u32[]{:S(2)}) copy-start(bf16[16,2048]{1,0:T(8,128)(2,1)} %param.23) | copy-start | bytes 196612
  7.2 18.4 %copy-start.14 = (f32[4]{0:T(128)S(1)}, f32[4]{0:T(128)}, u32[]{:S(2)}) copy-start(f32[4]{0:T(128)} %param.32) | copy-start | bytes 52
  7.2 19.6 %copy-start.15 = (bf16[128]{0:T(256)(128)(2,1)S(1)}, bf16[128]{0:T(256)(128)(2,1)}, u32[]{:S(2)}) copy-start(bf16[128]{0:T(256)(128)(2,1)} %param.33) | copy-start | bytes 772
  7.2 93.9 %all-gather.3.cloned.1.call-start = ((), (), s32[]{:S(2)}) async-start(), calls=%async_computation.8 | async-start | bytes 6389760 | tf_op jit(solution)/shard_map/all_gather | solution.py:12
  11.1 105.3 %all-to-all-start = ((bf16[64,512,32]{1,2,0:T(8,128)(2,1)}), bf16[64,512,32]{1,2,0:T(8,128)(2,1)S(1)}, u32[]{:S(2)}, u32[]{:S(2)}) async-start(bf16[64,512,32]{1,2,0:T(8,128)(2,1)} %broadcast_in_dim.16), calls=%async_computation | async-start | bytes 4194304 | tf_op jit(solution)/shard_map/all_to_all | solution.py:21
  108.3 3.6 %copy-start.1 = (f32[16,4,128,128]{3,2,1,0:T(8,128)S(1)}, f32[16,4,128,128]{3,2,1,0:T(8,128)}, u32[]{:S(2)}) copy-start(f32[16,4,128,128]{3,2,1,0:T(8,128)} %param.34) | copy-start | bytes 12582916
  113.5 8.1 %copy-start.11 = (bf16[2048]{0:T(1024)(128)(2,1)S(1)}, bf16[2048]{0:T(1024)(128)(2,1)}, u32[]{:S(2)}) copy-start(bf16[2048]{0:T(1024)(128)(2,1)} %param.36) | copy-start | bytes 12292
  116.2 22.9 %copy-start.8 = (bf16[32,128]{1,0:T(8,128)(2,1)S(1)}, bf16[32,128]{1,0:T(8,128)(2,1)}, u32[]{:S(2)}) copy-start(bf16[32,128]{1,0:T(8,128)(2,1)} %param.43) | copy-start | bytes 24580
  116.2 22.9 %copy-start.9 = (bf16[32,128]{1,0:T(8,128)(2,1)S(1)}, bf16[32,128]{1,0:T(8,128)(2,1)}, u32[]{:S(2)}) copy-start(bf16[32,128]{1,0:T(8,128)(2,1)} %param.42) | copy-start | bytes 24580
  116.2 40.5 %copy-start.5 = (bf16[128,32]{0,1:T(8,128)(2,1)S(1)}, bf16[128,32]{0,1:T(8,128)(2,1)}, u32[]{:S(2)}) copy-start(bf16[128,32]{0,1:T(8,128)(2,1)} %param.44) | copy-start | bytes 24580
  116.2 47.1 %copy-start.12 = (bf16[2048]{0:T(1024)(128)(2,1)S(1)}, bf16[2048]{0:T(1024)(128)(2,1)}, u32[]{:S(2)}) copy-start(bf16[2048]{0:T(1024)(128)(2,1)} %param.45) | copy-start | bytes 12292
  116.2 47.1 %copy-start.7 = (f32[16,4]{0,1:T(4,128)S(1)}, f32[16,4]{0,1:T(4,128)}, u32[]{:S(2)}) copy-start(f32[16,4]{0,1:T(4,128)} %param.38) | copy-start | bytes 772
  116.4 47.1 %copy-start.3 = (bf16[1,2048,128]{2,1,0:T(8,128)(2,1)S(1)}, bf16[1,2048,128]{2,1,0:T(8,128)(2,1)}, u32[]{:S(2)}) copy-start(bf16[1,2048,128]{2,1,0:T(8,128)(2,1)} %param.39) | copy-start | bytes 1572868
  117.8 9.8 %all-to-all-start.1 = ((bf16[4,16,2048]{2,1,0:T(8,128)(2,1)}), bf16[4,16,2048]{2,1,0:T(8,128)(2,1)S(1)}, u32[]{:S(2)}, u32[]{:S(2)}) async-start(bf16[4,16,2048]{2,1,0:T(8,128)(2,1)} %broadcast_in_dim.17), calls=%async_computation.1 | async-start | bytes 524288 | tf_op jit(solution)/shard_map/all_to_all | solution.py:21
  129.3 27.4 %all-to-all-start.2 = ((bf16[64,2,2048]{2,1,0:T(2,128)(2,1)}), bf16[64,2,2048]{2,1,0:T(2,128)(2,1)S(1)}, u32[]{:S(2)}, u32[]{:S(2)}) async-start(bf16[64,2,2048]{2,1,0:T(2,128)(2,1)} %reshape.147), calls=%async_computation.2 | async-start | bytes 1048576 | tf_op jit(solution)/shard_map/all_to_all | solution.py:184
  139.0 80.6 %all-gather.5.cloned.1.call-start = ((), (), s32[]{:S(2)}) async-start(), calls=%async_computation.9 | async-start | bytes 1064960 | tf_op jit(solution)/shard_map/all_gather | solution.py:12
  157.6 23.7 %all-to-all-start.5 = ((bf16[64,128,32]{1,2,0:T(8,128)(2,1)}), bf16[64,128,32]{1,2,0:T(8,128)(2,1)S(1)}, u32[]{:S(2)}, u32[]{:S(2)}) async-start(bf16[64,128,32]{1,2,0:T(8,128)(2,1)} %broadcast_in_dim.18), calls=%async_computation.5 | async-start | bytes 1048576 | tf_op jit(solution)/shard_map/all_to_all | solution.py:21
  181.3 41.1 %all-to-all-start.3 = ((bf16[4,128,512]{2,1,0:T(8,128)(2,1)}), bf16[4,128,512]{2,1,0:T(8,128)(2,1)S(1)}, u32[]{:S(2)}, u32[]{:S(2)}) async-start(bf16[4,128,512]{2,1,0:T(8,128)(2,1)} %bitcast.66), calls=%async_computation.3 | async-start | bytes 1048576 | tf_op jit(solution)/shard_map/all_to_all | solution.py:48
  223.1 9.9 %all-to-all-start.6 = ((bf16[4,16,2048]{2,1,0:T(8,128)(2,1)}), bf16[4,16,2048]{2,1,0:T(8,128)(2,1)S(1)}, u32[]{:S(2)}, u32[]{:S(2)}) async-start(bf16[4,16,2048]{2,1,0:T(8,128)(2,1)} %broadcast_in_dim.19), calls=%async_computation.6 | async-start | bytes 524288 | tf_op jit(solution)/shard_map/all_to_all | solution.py:21
  233.0 19.3 %all-to-all-start.4 = ((bf16[64,2,512]{2,1,0:T(2,128)(2,1)}), bf16[64,2,512]{2,1,0:T(2,128)(2,1)S(1)}, u32[]{:S(2)}, u32[]{:S(2)}) async-start(bf16[64,2,512]{2,1,0:T(2,128)(2,1)} %reshape.150), calls=%async_computation.4 | async-start | bytes 262144 | tf_op jit(solution)/shard_map/all_to_all | solution.py:195
  (1 other events, 2.0 us)
Sparse Core Ops, SparseCore 0:
  11.4 89.7 all-gather.2
  143.2 76.4 all-gather.4
where the time goes:
time: 268 us; the launch traced here: 267 us
  waiting for transfers between devices  163 us (61%)
  starting transfers between devices  48.1 us (18%)
  matrix products  19 us (7%)
  between operations  14.6 us (5%)
  local copies, waits for them, and re-layouts  10.9 us (4%)
  blocking collectives  6.84 us (3%)
  other arithmetic  4.85 us (2%)
    all_gather x2, waiting for transfers between devices, side_by_side(): whole, at, outs = (lax.all_gather(both, axis, axis=dim, tiled=True), 0, [])  109 us
    all_to_all x4, starting transfers between devices, copy_for_each(): return lax.all_to_all(copies, axis, split_axis=0, concat_axis=0, tiled=True)  26.7 us
    all_to_all x4, waiting for transfers between devices, copy_for_each(): return lax.all_to_all(copies, axis, split_axis=0, concat_axis=0, tiled=True)  25.9 us
    all_to_all x1, waiting for transfers between devices, per_device(): lax.all_to_all(outgoing, 'ep', split_axis=0, concat_axis=0, tiled=True)  16.9 us
    all_to_all x1, waiting for transfers between devices, per_device(): lax.all_to_all(part_cols.reshape(received.shape[0], received.shape[1], sh...  10.8 us
    all_to_all x1, starting transfers between devices, per_device(): lax.all_to_all(outgoing, 'ep', split_axis=0, concat_axis=0, tiled=True)  9.74 us
    all_to_all x1, starting transfers between devices, per_device(): lax.all_to_all(part_cols.reshape(received.shape[0], received.shape[1], sh...  8.16 us
    dot_general x4, matrix products, per_device(): jnp.dot(token_block, weight_piece, preferred_element_type=jnp.float32)  7.1 us
  transfers between devices with their start and end apart: 9, of which 7 were waited for; matrix products, arithmetic and copies ran while one was open for 10% of the time, Pallas kernels for 0%

commit v1 on v0

v1 whole, which is shorter than its diff:
```python
import jax
import jax.numpy as jnp
from jax import lax
from jax.sharding import Mesh
from jax.sharding import PartitionSpec as P

EPS = 1e-06
ROUTED_SCALE = 2.5
BF = jnp.bfloat16
F32 = jnp.float32


def rms_scale(values, gain):
    values = values.astype(F32)
    return (
        values
        * lax.rsqrt(jnp.mean(values * values, axis=-1, keepdims=True) + EPS)
        * gain.astype(F32)
    )


def unit_rows(values):
    return values * lax.rsqrt(jnp.sum(values * values, axis=-1, keepdims=True) + EPS)


def exchange(pieces, axis):
    return lax.all_to_all(pieces, axis, split_axis=0, concat_axis=0, tiled=True)


def copies(array, axis):
    return jnp.broadcast_to(array, (lax.axis_size(axis), *array.shape))


def dot(a, b):
    return jnp.dot(a, b, preferred_element_type=F32)


def rows_from_all(piece):
    over_z = exchange(copies(piece, "z"), "z")
    over_y = exchange(copies(over_z, "y"), "y")
    other = lax.ppermute(over_y, "c", [(0, 1), (1, 0)])
    first = lax.axis_index("c") == 0
    both = jnp.stack([jnp.where(first, over_y, other), jnp.where(first, other, over_y)])
    return both.transpose(2, 1, 0, 3, 4).reshape(-1, piece.shape[1])


def per_device(
    tokens,
    norm_gain,
    query_weight,
    key_weight,
    value_weight,
    outgate_weight,
    beta_weight,
    decay_weight,
    decay_rate,
    decay_bias,
    head_gain,
    recurrent,
    output_weight,
    ffn_gain,
    routes,
    route_weight,
    expert_gate,
    expert_up,
    expert_down,
    shared_gate,
    shared_up,
    shared_down,
    branch_gate,
):
    nz, ny, nc = lax.axis_size("z"), lax.axis_size("y"), lax.axis_size("c")
    ep_count = nz * ny * nc
    seq_local, width = tokens.shape
    heads_local, key_dim, value_dim = recurrent.shape[1:]
    rows_k = query_weight.shape[0]
    block_k = ny * nc * rows_k

    weights = jnp.concatenate((query_weight, key_weight, value_weight, outgate_weight), axis=1)
    over_y = exchange(copies(weights, "y"), "y")
    normed = rms_scale(tokens, norm_gain).astype(BF)
    at = jnp.arange(block_k)
    src = (at // rows_k % ny) * (nc * rows_k) + (at // (rows_k * ny)) * rows_k + at % rows_k
    perm = (jnp.arange(block_k)[:, None] == src[None, :]).astype(BF)
    blocks = normed.reshape(seq_local, nz, block_k).transpose(1, 0, 2).reshape(nz * seq_local, block_k)
    blocks = dot(blocks, perm).astype(BF).reshape(nz, seq_local, block_k)
    arrived = exchange(blocks, "z").reshape(nz * seq_local, block_k)
    block_weights = lax.all_gather(over_y, "c", axis=0).reshape(block_k, weights.shape[1])
    partial = dot(arrived, block_weights).astype(BF).reshape(nz, seq_local, -1)
    proj = exchange(partial, "z").astype(F32).sum(axis=0).astype(BF).astype(F32)

    out_rows = rows_from_all(output_weight.T)
    shared_piece = jnp.concatenate((shared_gate, shared_up, shared_down.T), axis=1)
    shared_rows = rows_from_all(shared_piece)

    head_start = lax.axis_index("x") * heads_local
    beta_logit = dot(normed, lax.dynamic_slice_in_dim(beta_weight, head_start, heads_local, 1))
    decay_logit = dot(normed, lax.dynamic_slice_in_dim(decay_weight, head_start, heads_local, 1))
    strength = jax.nn.sigmoid(beta_logit)
    retain = jnp.exp(-decay_rate[None, :] * jax.nn.softplus(decay_logit + decay_bias[None, :]))

    nq, nv = query_weight.shape[1], value_weight.shape[1]
    key_local = nq // key_dim
    repeat_count = heads_local // key_local
    silu = jax.nn.silu(proj)
    queries = unit_rows(silu[:, :nq].reshape(seq_local, key_local, key_dim))
    queries = jnp.repeat(queries, repeat_count, axis=1) * key_dim ** (-0.5)
    key_rows = unit_rows(silu[:, nq : 2 * nq].reshape(seq_local, key_local, key_dim))
    key_rows = jnp.repeat(key_rows, repeat_count, axis=1)
    value_rows = silu[:, 2 * nq : 2 * nq + nv].reshape(seq_local, heads_local, value_dim)
    out_gate = silu[:, 2 * nq + nv :].reshape(seq_local, heads_local, value_dim)

    decayed = recurrent * retain[:, :, None, None]
    predicted = jnp.einsum("shde,shd->she", decayed, key_rows)
    correction = strength[:, :, None] * (value_rows - predicted)
    new_state = decayed + key_rows[:, :, :, None] * correction[:, :, None, :]
    readout = jnp.einsum("shde,shd->she", new_state, queries)
    heads_out = (
        (rms_scale(readout, head_gain) * out_gate)
        .astype(BF)
        .reshape(seq_local, heads_local * value_dim)
    )
    partial_mix = lax.dot_general(
        heads_out, out_rows, (((1,), (1,)), ((), ())), preferred_element_type=F32
    ).astype(BF)
    mixed = exchange(copies(partial_mix, "x"), "x").astype(F32).sum(axis=0)
    residual = (tokens.astype(F32) + mixed).astype(BF)
    ffn_in = rms_scale(residual, ffn_gain).astype(BF)

    topk = routes.shape[1]
    pair_count = seq_local * topk
    capacity = 2 * ((pair_count + ep_count - 1) // ep_count)
    expert_ids = routes.reshape(pair_count)
    onehot = (expert_ids[:, None] == jnp.arange(ep_count)[None, :]).astype(F32)
    earlier = (jnp.arange(pair_count)[:, None] > jnp.arange(pair_count)[None, :]).astype(F32)
    slots = jnp.sum(jnp.dot(earlier, onehot) * onehot, axis=1).astype(jnp.int32)
    target = (expert_ids * capacity + slots).reshape(seq_local, topk)
    place = target[:, :, None] == jnp.arange(ep_count * capacity)[None, None, :]
    scaled = route_weight / jnp.sum(route_weight, axis=1, keepdims=True) * ROUTED_SCALE
    dispatch = jnp.any(place, axis=1).astype(BF)
    combine = jnp.sum(jnp.where(place, scaled[:, :, None], 0.0), axis=1)
    combine_high = combine.astype(BF)
    combine_low = (combine - combine_high.astype(F32)).astype(BF)

    outgoing = dot(dispatch.T, ffn_in).astype(BF).reshape(ep_count, capacity, width)
    received = exchange(outgoing, ("z", "y", "c")).reshape(-1, width)
    act = (jax.nn.silu(dot(received, expert_gate[0])) * dot(received, expert_up[0])).astype(BF)
    partial_rows = dot(act, expert_down[0]).astype(BF).reshape(ep_count, capacity, width)
    returned = exchange(partial_rows, ("z", "y", "c")).reshape(-1, width)

    hidden = shared_gate.shape[1]
    shared_g = dot(ffn_in, shared_rows[:, :hidden])
    shared_u = dot(ffn_in, shared_rows[:, hidden : 2 * hidden])
    shared_act = (jax.nn.silu(shared_g) * shared_u).astype(BF)
    shared_part = lax.dot_general(
        shared_act, shared_rows[:, 2 * hidden :], (((1,), (1,)), ((), ())), preferred_element_type=F32
    )
    branch = jax.nn.sigmoid(dot(ffn_in, branch_gate))

    moe = dot(jnp.concatenate((combine_high, combine_low), axis=0), returned)
    moe = moe[:seq_local] + moe[seq_local:]
    addend = (moe + branch[:, None] * shared_part).astype(BF)
    summed = exchange(copies(addend, "x"), "x").astype(F32).sum(axis=0)
    layer_out = (residual.astype(F32) + summed).astype(BF)
    return (layer_out, new_state)


def solution(mesh):
    ep, tp = mesh.devices.shape
    fine = Mesh(mesh.devices.reshape(ep // 8, 4, 2, tp), ("z", "y", "c", "x"))
    E = ("z", "y", "c")
    return jax.shard_map(
        per_device,
        mesh=fine,
        in_specs=(
            P(E, None),
            P(),
            P(E, "x"),
            P(E, "x"),
            P(E, "x"),
            P(E, "x"),
            P(),
            P(),
            P("x"),
            P("x"),
            P(),
            P(E, "x", None, None),
            P("x", E),
            P(),
            P(E, None),
            P(E, None),
            P(E, None, "x"),
            P(E, None, "x"),
            P(E, "x", None),
            P(E, "x"),
            P(E, "x"),
            P("x", E),
            P(),
        ),
        out_specs=(P(E, None), P(E, "x", None, None)),
        check_vma=False,
    )
```

time: 268 us -> 183 us (0.68)
  waiting for transfers between devices: 163 us -> 65.4 us
  blocking collectives: 6.84 us -> 24.5 us
  between operations: 14.6 us -> 1.21 us
  starting transfers between devices: 48.1 us -> 57.1 us
  other arithmetic: 4.85 us -> 9.95 us
  matrix products: 19 us -> 14.7 us
    all_gather x2 -> x0, waiting for transfers between devices: 109 us -> none  [side_by_side(): whole, at, outs = (lax.all_gather(both, axis, axis=dim, tiled=True), 0, [])]
    all_to_all x1 -> x2, blocking collectives: 6.84 us -> 19 us  [exchange(): return lax.all_to_all(pieces, axis, split_axis=0, concat_axis=0, tiled=True)]
    all_to_all x7 -> x9, waiting for transfers between devices: 53.7 us -> 65.4 us  [exchange(): return lax.all_to_all(pieces, axis, split_axis=0, concat_axis=0, tiled=True)]
    ppermute x0 -> x2, starting transfers between devices: none -> 6.76 us  [rows_from_all(): other = lax.ppermute(over_y, 'c', [(0, 1), (1, 0)])]
    dot_general x14 -> x12, matrix products: 15.1 us -> 8.64 us  [the longest x10 7.53 us: dot(): return jnp.dot(a, b, preferred_element_type=F32)]
    all_gather x0 -> x1, blocking collectives: none -> 5.52 us  [per_device(): lax.all_gather(over_y, 'c', axis=0).reshape(block_k, weights.shape[1])]
    all_to_all x7 -> x9, starting transfers between devices: 48 us -> 50.4 us  [exchange(): return lax.all_to_all(pieces, axis, split_axis=0, concat_axis=0, tiled=True)]
  transfers between devices with their start and end apart: 9 -> 11, of which waited for: 7 -> 8; matrix products, arithmetic and copies ran while one was open for 10% -> 13% of each run, Pallas kernels for 0% -> 0%
where the time goes in v1:
time: 183 us; the launch traced here: 182 us
  waiting for transfers between devices  65.4 us (36%)
  starting transfers between devices  57.1 us (31%)
  blocking collectives  24.5 us (13%)
  matrix products  14.7 us (8%)
  other arithmetic  9.95 us (5%)
  local copies, waits for them, and re-layouts  8.72 us (5%)
    all_to_all x9, waiting for transfers between devices, exchange(): return lax.all_to_all(pieces, axis, split_axis=0, concat_axis=0, tiled=True)  65.4 us
    all_to_all x9, starting transfers between devices, exchange(): return lax.all_to_all(pieces, axis, split_axis=0, concat_axis=0, tiled=True)  50.4 us
    all_to_all x2, blocking collectives, exchange(): return lax.all_to_all(pieces, axis, split_axis=0, concat_axis=0, tiled=True)  19 us
    dot_general x10, matrix products, dot(): return jnp.dot(a, b, preferred_element_type=F32)  7.53 us
    ppermute x2, starting transfers between devices, rows_from_all(): other = lax.ppermute(over_y, 'c', [(0, 1), (1, 0)])  6.76 us
    all_gather x1, blocking collectives, per_device(): lax.all_gather(over_y, 'c', axis=0).reshape(block_k, weights.shape[1])  5.52 us
    broadcast_in_dim x7, local copies, waits for them, and re-layouts, copies(): return jnp.broadcast_to(array, (lax.axis_size(axis), *array.shape))  5 us
  transfers between devices with their start and end apart: 11, of which 8 were waited for; matrix products, arithmetic and copies ran while one was open for 13% of the time, Pallas kernels for 0%

profile of v1, /device:TPU:1, one launch (start us, length us, event | category | flops | bytes accessed | tf_op | source)
XLA Modules:
  0.0 181.6 jit_solution(16361960758001976967)
XLA Ops:
  4.3 9.0 %all-to-all-start = ((bf16[8,16,256]{2,1,0:T(8,128)(2,1)}), bf16[8,16,256]{2,1,0:T(8,128)(2,1)S(1)}, u32[]{:S(2)}, u32[]{:S(2)}) async-start(bf16[8,16,256]{2,1,0:T(8,128)(2,1)} %bitcast.2), calls=%async_computation | async-start | bytes 131072 | tf_op jit(solution)/shard_map/all_to_all | solution.py:27
  14.1 6.4 %all-to-all-done = bf16[8,16,256]{2,1,0:T(8,128)(2,1)S(1)} async-done(((bf16[8,16,256]{2,1,0:T(8,128)(2,1)}), bf16[8,16,256]{2,1,0:T(8,128)(2,1)S(1)}, u32[]{:S(2)}, u32[]{:S(2)}) %all-to-all-start) | async-done | bytes 65568 | tf_op jit(solution)/shard_map/all_to_all | solution.py:27
  20.5 10.2 %all_to_all.55 = bf16[4,32,1536]{2,1,0:T(8,128)(2,1)S(1)} all-to-all(bf16[4,32,1536]{2,1,0:T(8,128)(2,1)S(1)} %broadcast_in_dim.26), channel_id=1, replica_groups=mesh['z'=8,'y'=4,'c'=2,'x'=4] {'y'}, dimensions={0} | all-to-all | bytes 786432 | tf_op jit(solution)/shard_map/all_to_all | solution.py:27
  32.2 3.4 %all-to-all-start.3 = ((bf16[8,32,512]{2,1,0:T(8,128)(2,1)}), bf16[8,32,512]{2,1,0:T(8,128)(2,1)S(1)}, u32[]{:S(2)}, u32[]{:S(2)}) async-start(bf16[8,32,512]{2,1,0:T(8,128)(2,1)} %broadcast_in_dim.29), calls=%async_computation.3 | async-start | bytes 524288 | tf_op jit(solution)/shard_map/all_to_all | solution.py:27
  35.6 5.5 %all-gather = bf16[8,32,1536]{2,1,0:T(8,128)(2,1)S(1)} all-gather(bf16[4,32,1536]{2,1,0:T(8,128)(2,1)S(1)} %all_to_all.55), channel_id=2, replica_groups=mesh['z'=8,'y'=4,'c'=2,'x'=4] {'c'}, dimensions={0}, use_global_device_ids=true | all-gather | bytes 1179648 | tf_op jit(solution)/shard_map/all_gather | solution.py:88
  42.2 2.8 %all-to-all-done.3 = bf16[8,32,512]{2,1,0:T(8,128)(2,1)S(1)} async-done(((bf16[8,32,512]{2,1,0:T(8,128)(2,1)}), bf16[8,32,512]{2,1,0:T(8,128)(2,1)S(1)}, u32[]{:S(2)}, u32[]{:S(2)}) %all-to-all-start.3) | async-done | bytes 262176 | tf_op jit(solution)/shard_map/all_to_all | solution.py:27
  45.0 4.0 %all-to-all-start.2 = ((bf16[8,16,1536]{2,1,0:T(8,128)(2,1)}), bf16[8,16,1536]{2,1,0:T(8,128)(2,1)S(1)}, u32[]{:S(2)}, u32[]{:S(2)}) async-start(bf16[8,16,1536]{2,1,0:T(8,128)(2,1)} %bitcast.5), calls=%async_computation.2 | async-start | bytes 786432 | tf_op jit(solution)/shard_map/all_to_all | solution.py:27
  51.6 8.2 %all-to-all-done.2 = bf16[8,16,1536]{2,1,0:T(8,128)(2,1)S(1)} async-done(((bf16[8,16,1536]{2,1,0:T(8,128)(2,1)}), bf16[8,16,1536]{2,1,0:T(8,128)(2,1)S(1)}, u32[]{:S(2)}, u32[]{:S(2)}) %all-to-all-start.2) | async-done | bytes 393248 | tf_op jit(solution)/shard_map/all_to_all | solution.py:27
  60.9 3.5 %all-to-all-start.4 = ((bf16[4,8,32,512]{3,2,1,0:T(8,128)(2,1)}), bf16[4,8,32,512]{3,2,1,0:T(8,128)(2,1)S(1)}, u32[]{:S(2)}, u32[]{:S(2)}) async-start(bf16[4,8,32,512]{3,2,1,0:T(8,128)(2,1)} %broadcast_in_dim.30), calls=%async_computation.4 | async-start | bytes 2097152 | tf_op jit(solution)/shard_map/all_to_all | solution.py:27
  65.0 3.1 %fusion = f32[16,4,1,128]{3,2,1,0:T(1,128)S(1)} fusion(f32[16,4,128,1]{2,3,1,0:T(1,128)S(1)} %bitcast.85, f32[16,4,128,128]{3,2,1,0:T(8,128)} %param.34, f32[16,4]{1,0:T(8,128)S(1)} %copy.73), kind=kOutput, calls=%fused_computation.1 | convolution fusion | flops 3145728 | bytes 4260096 | tf_op jit(solution)/shard_map/shde,shd->she/dot_general | solution.py:114
  68.3 2.8 %multiply_add_fusion = f32[16,4,128,128]{3,2,1,0:T(8,128)} fusion(f32[16,4,128,128]{3,2,1,0:T(8,128)S(1)} %copy-done.1, f32[16,4,128]{2,1,0:T(4,128)S(1)} %subtract_multiply_fusion, f32[16,4,128]{2,1,0:T(4,128)S(1)} %bitcast.86, f32[16,4]{1,0:T(8,128)S(1)} %copy.73), kind=kLoop, calls=%fused_computation | loop fusion | flops 3145728 | bytes 8454400 | tf_op jit(solution)/shard_map/add | solution.py:116
  71.1 3.3 %all-to-all-done.4 = bf16[4,8,32,512]{3,2,1,0:T(8,128)(2,1)S(1)} async-done(((bf16[4,8,32,512]{3,2,1,0:T(8,128)(2,1)}), bf16[4,8,32,512]{3,2,1,0:T(8,128)(2,1)S(1)}, u32[]{:S(2)}, u32[]{:S(2)}) %all-to-all-start.4) | async-done | bytes 1048608 | tf_op jit(solution)/shard_map/all_to_all | solution.py:27
  75.0 3.4 %all-to-all-start.8 = ((bf16[8,32,384]{2,1,0:T(8,128)(2,1)}), bf16[8,32,384]{2,1,0:T(8,128)(2,1)S(1)}, u32[]{:S(2)}, u32[]{:S(2)}) async-start(bf16[8,32,384]{2,1,0:T(8,128)(2,1)} %broadcast_in_dim.38), calls=%async_computation.8 | async-start | bytes 393216 | tf_op jit(solution)/shard_map/all_to_all | solution.py:27
  78.5 6.2 %collective-permute-start = (bf16[4,8,32,512]{3,2,0,1:T(8,128)(2,1)S(1)}, bf16[4,8,32,512]{3,2,0,1:T(8,128)(2,1)S(1)}, u32[]{:S(2)}, u32[]{:S(2)}) collective-permute-start(bf16[4,8,32,512]{3,2,0,1:T(8,128)(2,1)S(1)} %copy.77), channel_id=1, source_target_pairs={{0,4},{4,0},{1,5},{5,1},{2,6},{6,2},{3,7},{7,3},{8,12},{12,8},{9,1... | collective-permute-start | bytes 3145736 | tf_op jit(solution)/shard_map/ppermute | solution.py:41
  84.8 2.8 %fusion.84 = f32[16,4,1,128]{3,2,1,0:T(1,128)S(1)} fusion(f32[16,4,128,128]{3,2,1,0:T(8,128)} %multiply_add_fusion, f32[16,4,128,1]{2,3,1,0:T(1,128)S(1)} %bitcast.93), kind=kOutput, calls=%fused_computation.138 | convolution fusion | flops 2097152 | bytes 4259840 | tf_op jit(solution)/shard_map/shde,shd->she/dot_general | solution.py:117
  89.8 4.0 %all-to-all-start.5 = ((bf16[4,16,2048]{2,1,0:T(8,128)(2,1)}), bf16[4,16,2048]{2,1,0:T(8,128)(2,1)S(1)}, u32[]{:S(2)}, u32[]{:S(2)}) async-start(bf16[4,16,2048]{2,1,0:T(8,128)(2,1)} %broadcast_in_dim.31), calls=%async_computation.5 | async-start | bytes 524288 | tf_op jit(solution)/shard_map/all_to_all | solution.py:27
  93.9 5.4 %all-to-all-done.5 = bf16[4,16,2048]{2,1,0:T(8,128)(2,1)S(1)} async-done(((bf16[4,16,2048]{2,1,0:T(8,128)(2,1)}), bf16[4,16,2048]{2,1,0:T(8,128)(2,1)S(1)}, u32[]{:S(2)}, u32[]{:S(2)}) %all-to-all-start.5) | async-done | bytes 262176 | tf_op jit(solution)/shard_map/all_to_all | solution.py:27
  100.3 3.5 %all-to-all-start.9 = ((bf16[4,8,32,384]{3,2,1,0:T(8,128)(2,1)}), bf16[4,8,32,384]{3,2,1,0:T(8,128)(2,1)S(1)}, u32[]{:S(2)}, u32[]{:S(2)}) async-start(bf16[4,8,32,384]{3,2,1,0:T(8,128)(2,1)} %broadcast_in_dim.70), calls=%async_computation.9 | async-start | bytes 1572864 | tf_op jit(solution)/shard_map/all_to_all | solution.py:27
  105.5 6.6 %all-to-all-done.9 = bf16[4,8,32,384]{3,2,1,0:T(8,128)(2,1)S(1)} async-done(((bf16[4,8,32,384]{3,2,1,0:T(8,128)(2,1)}), bf16[4,8,32,384]{3,2,1,0:T(8,128)(2,1)S(1)}, u32[]{:S(2)}, u32[]{:S(2)}) %all-to-all-start.9) | async-done | bytes 786464 | tf_op jit(solution)/shard_map/all_to_all | solution.py:27
  112.1 13.8 %all-to-all-start.6 = ((bf16[64,2,2048]{2,1,0:T(2,128)(2,1)}), bf16[64,2,2048]{2,1,0:T(2,128)(2,1)S(1)}, u32[]{:S(2)}, u32[]{:S(2)}) async-start(bf16[64,2,2048]{2,1,0:T(2,128)(2,1)} %reshape.173), calls=%async_computation.6 | async-start | bytes 1048576 | tf_op jit(solution)/shard_map/all_to_all | solution.py:27
  126.7 16.9 %all-to-all-done.6 = bf16[64,2,2048]{2,1,0:T(2,128)(2,1)S(1)} async-done(((bf16[64,2,2048]{2,1,0:T(2,128)(2,1)}), bf16[64,2,2048]{2,1,0:T(2,128)(2,1)S(1)}, u32[]{:S(2)}, u32[]{:S(2)}) %all-to-all-start.6) | async-done | bytes 524320 | tf_op jit(solution)/shard_map/all_to_all | solution.py:27
  147.9 5.7 %all-to-all-start.7 = ((bf16[64,2,2048]{2,1,0:T(2,128)(2,1)}), bf16[64,2,2048]{2,1,0:T(2,128)(2,1)S(1)}, u32[]{:S(2)}, u32[]{:S(2)}) async-start(bf16[64,2,2048]{2,1,0:T(2,128)(2,1)} %reshape.175), calls=%async_computation.7 | async-start | bytes 1048576 | tf_op jit(solution)/shard_map/all_to_all | solution.py:27
  155.6 15.7 %all-to-all-done.7 = bf16[64,2,2048]{2,1,0:T(2,128)(2,1)S(1)} async-done(((bf16[64,2,2048]{2,1,0:T(2,128)(2,1)}), bf16[64,2,2048]{2,1,0:T(2,128)(2,1)S(1)}, u32[]{:S(2)}, u32[]{:S(2)}) %all-to-all-start.7) | async-done | bytes 524320 | tf_op jit(solution)/shard_map/all_to_all | solution.py:27
  172.2 8.8 %all_to_all.56 = bf16[4,16,2048]{2,1,0:T(8,128)(2,1)S(1)} all-to-all(bf16[4,16,2048]{2,1,0:T(8,128)(2,1)S(1)} %broadcast_in_dim.71), channel_id=1, replica_groups=mesh['z'=8,'y'=4,'c'=2,'x'=4] {'x'}, dimensions={0} | all-to-all | bytes 524288 | tf_op jit(solution)/shard_map/all_to_all | solution.py:27
  (111 shorter events, 25.3 us)
Async XLA Ops:
  0.6 144.5 %copy-start = (bf16[1,128,2048]{2,1,0:T(8,128)(2,1)S(1)}, bf16[1,128,2048]{2,1,0:T(8,128)(2,1)}, u32[]{:S(2)}) copy-start(bf16[1,128,2048]{2,1,0:T(8,128)(2,1)} %param.41) | copy-start | bytes 1572868
  0.6 48.4 %copy-start.3 = (s32[16,4]{0,1:T(4,128)S(1)}, s32[16,4]{0,1:T(4,128)}, u32[]{:S(2)}) copy-start(s32[16,4]{0,1:T(4,128)} %param.37) | copy-start | bytes 772
  0.7 48.9 %copy-start.10 = (f32[4]{0:T(128)S(1)}, f32[4]{0:T(128)}, u32[]{:S(2)}) copy-start(f32[4]{0:T(128)} %param.31) | copy-start | bytes 52
  0.7 48.9 %copy-start.11 = (f32[4]{0:T(128)S(1)}, f32[4]{0:T(128)}, u32[]{:S(2)}) copy-start(f32[4]{0:T(128)} %param.32) | copy-start | bytes 52
  0.7 50.9 %copy-start.12 = (bf16[128]{0:T(256)(128)(2,1)S(1)}, bf16[128]{0:T(256)(128)(2,1)}, u32[]{:S(2)}) copy-start(bf16[128]{0:T(256)(128)(2,1)} %param.33) | copy-start | bytes 772
  0.7 50.9 %copy-start.5 = (bf16[128,32]{0,1:T(8,128)(2,1)S(1)}, bf16[128,32]{0,1:T(8,128)(2,1)}, u32[]{:S(2)}) copy-start(bf16[128,32]{0,1:T(8,128)(2,1)} %param.44) | copy-start | bytes 24580
  0.7 50.9 %copy-start.6 = (bf16[32,128]{1,0:T(8,128)(2,1)S(1)}, bf16[32,128]{1,0:T(8,128)(2,1)}, u32[]{:S(2)}) copy-start(bf16[32,128]{1,0:T(8,128)(2,1)} %param.43) | copy-start | bytes 24580
  0.7 50.9 %copy-start.7 = (bf16[32,128]{1,0:T(8,128)(2,1)S(1)}, bf16[32,128]{1,0:T(8,128)(2,1)}, u32[]{:S(2)}) copy-start(bf16[32,128]{1,0:T(8,128)(2,1)} %param.42) | copy-start | bytes 24580
  4.3 16.2 %all-to-all-start = ((bf16[8,16,256]{2,1,0:T(8,128)(2,1)}), bf16[8,16,256]{2,1,0:T(8,128)(2,1)S(1)}, u32[]{:S(2)}, u32[]{:S(2)}) async-start(bf16[8,16,256]{2,1,0:T(8,128)(2,1)} %bitcast.2), calls=%async_computation | async-start | bytes 131072 | tf_op jit(solution)/shard_map/all_to_all | solution.py:27
  32.2 12.8 %all-to-all-start.3 = ((bf16[8,32,512]{2,1,0:T(8,128)(2,1)}), bf16[8,32,512]{2,1,0:T(8,128)(2,1)S(1)}, u32[]{:S(2)}, u32[]{:S(2)}) async-start(bf16[8,32,512]{2,1,0:T(8,128)(2,1)} %broadcast_in_dim.29), calls=%async_computation.3 | async-start | bytes 524288 | tf_op jit(solution)/shard_map/all_to_all | solution.py:27
  45.0 14.9 %all-to-all-start.2 = ((bf16[8,16,1536]{2,1,0:T(8,128)(2,1)}), bf16[8,16,1536]{2,1,0:T(8,128)(2,1)S(1)}, u32[]{:S(2)}, u32[]{:S(2)}) async-start(bf16[8,16,1536]{2,1,0:T(8,128)(2,1)} %bitcast.5), calls=%async_computation.2 | async-start | bytes 786432 | tf_op jit(solution)/shard_map/all_to_all | solution.py:27
  60.9 13.4 %all-to-all-start.4 = ((bf16[4,8,32,512]{3,2,1,0:T(8,128)(2,1)}), bf16[4,8,32,512]{3,2,1,0:T(8,128)(2,1)S(1)}, u32[]{:S(2)}, u32[]{:S(2)}) async-start(bf16[4,8,32,512]{3,2,1,0:T(8,128)(2,1)} %broadcast_in_dim.30), calls=%async_computation.4 | async-start | bytes 2097152 | tf_op jit(solution)/shard_map/all_to_all | solution.py:27
  64.9 3.5 %copy-start.1 = (f32[16,4,128,128]{3,2,1,0:T(8,128)S(1)}, f32[16,4,128,128]{3,2,1,0:T(8,128)}, u32[]{:S(2)}) copy-start(f32[16,4,128,128]{3,2,1,0:T(8,128)} %param.34) | copy-start | bytes 12582916
  75.0 14.0 %all-to-all-start.8 = ((bf16[8,32,384]{2,1,0:T(8,128)(2,1)}), bf16[8,32,384]{2,1,0:T(8,128)(2,1)S(1)}, u32[]{:S(2)}, u32[]{:S(2)}) async-start(bf16[8,32,384]{2,1,0:T(8,128)(2,1)} %broadcast_in_dim.38), calls=%async_computation.8 | async-start | bytes 393216 | tf_op jit(solution)/shard_map/all_to_all | solution.py:27
  78.5 9.4 %collective-permute-start = (bf16[4,8,32,512]{3,2,0,1:T(8,128)(2,1)S(1)}, bf16[4,8,32,512]{3,2,0,1:T(8,128)(2,1)S(1)}, u32[]{:S(2)}, u32[]{:S(2)}) collective-permute-start(bf16[4,8,32,512]{3,2,0,1:T(8,128)(2,1)S(1)} %copy.77), channel_id=1, source_target_pairs={{0,4},{4,0},{1,5},{5,1},{2,6},{6,2},{3,7},{7,3},{8,12},{12,8},{9,1... | collective-permute-start | bytes 3145736 | tf_op jit(solution)/shard_map/ppermute | solution.py:41
  88.2 5.6 %copy-start.8 = (bf16[2048]{0:T(1024)(128)(2,1)S(1)}, bf16[2048]{0:T(1024)(128)(2,1)}, u32[]{:S(2)}) copy-start(bf16[2048]{0:T(1024)(128)(2,1)} %param.36) | copy-start | bytes 12292
  88.2 15.7 %copy-start.2 = (bf16[16,2048]{1,0:T(8,128)(2,1)S(1)}, bf16[16,2048]{1,0:T(8,128)(2,1)}, u32[]{:S(2)}) copy-start(bf16[16,2048]{1,0:T(8,128)(2,1)} %param.23) | copy-start | bytes 196612
  88.4 37.5 %copy-start.4 = (f32[16,4]{0,1:T(4,128)S(1)}, f32[16,4]{0,1:T(4,128)}, u32[]{:S(2)}) copy-start(f32[16,4]{0,1:T(4,128)} %param.38) | copy-start | bytes 772
  89.8 9.5 %all-to-all-start.5 = ((bf16[4,16,2048]{2,1,0:T(8,128)(2,1)}), bf16[4,16,2048]{2,1,0:T(8,128)(2,1)S(1)}, u32[]{:S(2)}, u32[]{:S(2)}) async-start(bf16[4,16,2048]{2,1,0:T(8,128)(2,1)} %broadcast_in_dim.31), calls=%async_computation.5 | async-start | bytes 524288 | tf_op jit(solution)/shard_map/all_to_all | solution.py:27
  100.3 11.8 %all-to-all-start.9 = ((bf16[4,8,32,384]{3,2,1,0:T(8,128)(2,1)}), bf16[4,8,32,384]{3,2,1,0:T(8,128)(2,1)S(1)}, u32[]{:S(2)}, u32[]{:S(2)}) async-start(bf16[4,8,32,384]{3,2,1,0:T(8,128)(2,1)} %broadcast_in_dim.70), calls=%async_computation.9 | async-start | bytes 1572864 | tf_op jit(solution)/shard_map/all_to_all | solution.py:27
  112.1 31.5 %all-to-all-start.6 = ((bf16[64,2,2048]{2,1,0:T(2,128)(2,1)}), bf16[64,2,2048]{2,1,0:T(2,128)(2,1)S(1)}, u32[]{:S(2)}, u32[]{:S(2)}) async-start(bf16[64,2,2048]{2,1,0:T(2,128)(2,1)} %reshape.173), calls=%async_computation.6 | async-start | bytes 1048576 | tf_op jit(solution)/shard_map/all_to_all | solution.py:27
  126.0 27.7 %copy-start.9 = (bf16[2048]{0:T(1024)(128)(2,1)S(1)}, bf16[2048]{0:T(1024)(128)(2,1)}, u32[]{:S(2)}) copy-start(bf16[2048]{0:T(1024)(128)(2,1)} %param.45) | copy-start | bytes 12292
  126.1 27.5 %collective-permute-start.1 = (bf16[4,8,32,384]{3,2,0,1:T(8,128)(2,1)S(1)}, bf16[4,8,32,384]{3,2,0,1:T(8,128)(2,1)}, u32[]{:S(2)}, u32[]{:S(2)}) collective-permute-start(bf16[4,8,32,384]{3,2,0,1:T(8,128)(2,1)S(1)} %copy.83), channel_id=1, source_target_pairs={{0,4},{4,0},{1,5},{5,1},{2,6},{6,2},{3,7},{7,3},{8,12},{12,8},{9,1... | collective-permute-start | bytes 2359304 | tf_op jit(solution)/shard_map/ppermute | solution.py:41
  147.9 23.4 %all-to-all-start.7 = ((bf16[64,2,2048]{2,1,0:T(2,128)(2,1)}), bf16[64,2,2048]{2,1,0:T(2,128)(2,1)S(1)}, u32[]{:S(2)}, u32[]{:S(2)}) async-start(bf16[64,2,2048]{2,1,0:T(2,128)(2,1)} %reshape.175), calls=%async_computation.7 | async-start | bytes 1048576 | tf_op jit(solution)/shard_map/all_to_all | solution.py:27
